TPU v7x, 512 devices: a whole 4x4x16 slice. The times are simulated.
512 devices in a mesh: sp: 32 (over z, core), tp: 16 (over y, x).
Axes of the slice: x: 4, y: 4, z: 16, core: 2. Of those that a mesh axis runs over, the one named last changes fastest.
Arguments:
- residual: bfloat16 [8192, 2048], P('sp'), may hold values from -6 to 6
- queries: bfloat16 [8192, 16, 128], P('sp', 'tp'), may hold values from -256 to 256
- key_vectors: bfloat16 [8192, 16, 128], P('sp', 'tp'), may hold values from -5.3 to 5.3
- value_rows: bfloat16 [8192, 16, 128], P('sp', 'tp'), may hold values from -6 to 6
- head_lambda: float32 [16], P('tp'), may hold values from 0.3 to 0.8
- head_gain: float32 [128], replicated, may hold values from 0.1 to 1.9
- out_weight: bfloat16 [2048, 2048], P('tp'), may hold values from -0.125 to 0.125
- ffn_gain: float32 [2048], replicated, may hold values from 0.1 to 1.9
- expert_gate: bfloat16 [32, 2048, 4096], P('sp', None, 'tp'), may hold values from -0.125 to 0.125
- expert_up: bfloat16 [32, 2048, 4096], P('sp', None, 'tp'), may hold values from -0.125 to 0.125
- expert_down: bfloat16 [32, 4096, 2048], P('sp', None, 'tp'), may hold values from -0.09375 to 0.09375
- routing: int32 [8192, 2], P('sp'), may hold values from 0 to 31, as said below
- route_weight: float32 [8192, 2], P('sp'), may hold values from 0.1 to 0.9
Outputs:
- layer_out: bfloat16 [8192, 2048], P('sp')
Inputs may be any that keep to these rules, and one draw needn't show every extreme that they name: `routing`: each row names two different experts of one group of 8 consecutive experts. In each aligned block of 256 rows no expert is named by more than 32 rows, and in every block some expert is named by exactly 32 rows.
All inputs are finite; a program needn't handle non-finite values.
Results may differ from a plain program's by a relative error of at most 0.015.
Values may be sent and summed in bfloat16 or wider, within the bound.
No kernel may reach another device: no remote copies, remote signals or barrier semaphores. Data moves between devices by JAX's collectives and lax.ppermute only.
A program may use at most 64 MiB of HBM per device.

v0:
```python
import math
import jax
import jax.numpy as jnp
from jax import lax
from jax.sharding import PartitionSpec as P

GROUPS = 4
norm_eps = 1e-06


def sent_together(arrays, axis, dim, along):
    ends, at = ([], 0)
    for a in arrays[:-1]:
        at += a.shape[along]
        ends.append(at)
    both = jnp.concatenate(arrays, axis=along)
    return tuple(jnp.split(lax.all_gather(both, axis, axis=dim, tiled=True), ends, axis=along))


def in_blocks(array, dim, peers):
    before, after = (array.shape[:dim], array.shape[dim + 1 :])
    return jnp.moveaxis(array.reshape(*before, peers, -1, *after), dim, 0)


def sum_at_owner(array, axis, dim):
    parts = in_blocks(array, dim, lax.axis_size(axis))
    arrived = lax.all_to_all(parts, axis, split_axis=0, concat_axis=0, tiled=True)
    return arrived.astype(jnp.float32).sum(axis=0)


def padded_to(lines, peers):
    spare = -len(lines) % peers
    return jnp.pad(lines, [(0, spare)] + [(0, 0)] * (lines.ndim - 1))


def from_everyone(array, axis):
    peers = lax.axis_size(axis)
    return lax.all_to_all(
        jnp.broadcast_to(array[None], (peers, *array.shape)), axis, 0, 0, tiled=True
    )


def laid_out(parts, dim):
    parts = jnp.moveaxis(parts, 0, dim)
    dims = parts.shape
    return parts.reshape(*dims[:dim], dims[dim] * dims[dim + 1], *dims[dim + 2 :])


def collect(array, axis, dim):
    parts = from_everyone(array, axis)
    return laid_out(parts, dim)


def sum_by_parts(array, axes):
    lines = array.reshape(-1, array.shape[-1])
    own = sum_at_owner(padded_to(lines, lax.axis_size(axes)), axes, 0)
    whole = collect(own.astype(jnp.bfloat16), axes, 0)
    return whole[: len(lines)].reshape(array.shape).astype(jnp.float32)


def online_update(running, query_part, key_part, value_part, query_pos, key_pos, score_scale):
    highest, totals, accum = running
    scores = (
        jnp.einsum("qhd,khd->hqk", query_part, key_part, preferred_element_type=jnp.float32)
        * score_scale
    )
    scores = jnp.where(key_pos[None, None, :] <= query_pos[None, :, None], scores, -jnp.inf)
    new_high = jnp.maximum(highest, jnp.max(scores, axis=-1))
    shrink = jnp.exp(highest - new_high)
    weights = jnp.exp(scores - new_high[:, :, None])
    totals = shrink * totals + jnp.sum(weights, axis=-1)
    blended = jnp.einsum(
        "hqk,khe->qhe", weights.astype(jnp.bfloat16), value_part, preferred_element_type=jnp.float32
    )
    accum = jnp.transpose(shrink)[:, :, None] * accum + blended
    return (new_high, totals, accum)


def shards(
    residual,
    queries,
    key_vectors,
    value_rows,
    head_lambda,
    head_gain,
    out_weight,
    ffn_gain,
    expert_gate,
    expert_up,
    expert_down,
    routing,
    route_weight,
):
    tok_count = queries.shape[0]
    local_heads = queries.shape[1]
    half_width = queries.shape[2] // 2
    value_width = value_rows.shape[2]
    score_scale = half_width ** (-0.5)
    query_pos = lax.axis_index("sp") * tok_count + jnp.arange(tok_count, dtype=jnp.int32)
    last_query = query_pos[-1]
    first_half = queries[:, :, :half_width]
    second_half = queries[:, :, half_width:]
    start_high = jnp.full((local_heads, tok_count), -1e30, jnp.float32)
    start_total = jnp.zeros((local_heads, tok_count), jnp.float32)
    start_accum = jnp.zeros((tok_count, local_heads, value_width), jnp.float32)
    empty_state = (start_high, start_total, start_accum)
    running = (empty_state, empty_state)
    key_piece, value_piece = sent_together((key_vectors, value_rows), "sp", 0, 1)
    piece_len = key_piece.shape[0]
    block_len = math.gcd(piece_len, 512)
    block_count = piece_len // block_len
    key_blocks = key_piece.reshape(block_count, block_len, local_heads, 2 * half_width)
    value_blocks = value_piece.reshape(block_count, block_len, local_heads, value_width)

    def visit(current, stacked):
        block_index, key_block, value_block = stacked
        block_first = block_index * block_len
        key_pos = block_first + jnp.arange(block_len, dtype=jnp.int32)

        def compute(inside):
            first_state = online_update(
                inside[0],
                first_half,
                key_block[:, :, :half_width],
                value_block,
                query_pos,
                key_pos,
                score_scale,
            )
            second_state = online_update(
                inside[1],
                second_half,
                key_block[:, :, half_width:],
                value_block,
                query_pos,
                key_pos,
                score_scale,
            )
            return (first_state, second_state)

        return (lax.cond(block_first <= last_query, compute, lambda inside: inside, current), None)

    running, _ = lax.scan(
        visit, running, (jnp.arange(block_count, dtype=jnp.int32), key_blocks, value_blocks)
    )
    first_state, second_state = running
    first_out = first_state[2] / jnp.transpose(first_state[1])[:, :, None]
    second_out = second_state[2] / jnp.transpose(second_state[1])[:, :, None]
    combined = first_out - head_lambda[None, :, None] * second_out
    normed_heads = (
        combined
        * lax.rsqrt(jnp.mean(combined * combined, axis=-1, keepdims=True) + norm_eps)
        * head_gain
    )
    attended = normed_heads.astype(jnp.bfloat16).reshape(tok_count, local_heads * value_width)
    partial_proj = jnp.dot(attended, out_weight, preferred_element_type=jnp.float32)
    projected = sum_by_parts(partial_proj.astype(jnp.bfloat16), "tp")
    stream = residual.astype(jnp.float32) + projected
    block_normed = (
        stream * lax.rsqrt(jnp.mean(stream * stream, axis=-1, keepdims=True) + norm_eps) * ffn_gain
    ).astype(jnp.bfloat16)
    expert_count = lax.axis_size("sp")
    tp_count = lax.axis_size("tp")
    per_group = expert_count // GROUPS
    capacity = tok_count // per_group
    top_count = routing.shape[1]
    model_width = block_normed.shape[1]
    flat_routes = routing.reshape(-1)
    route_count = flat_routes.shape[0]
    onehot = (flat_routes[:, None] == jnp.arange(expert_count, dtype=jnp.int32)[None, :]).astype(
        jnp.int32
    )
    earlier = jnp.cumsum(onehot, axis=0) - onehot
    position = jnp.sum(earlier * onehot, axis=1)
    slot_index = flat_routes * capacity + position
    slot_token = (
        jnp.full((expert_count * capacity,), tok_count, jnp.int32)
        .at[slot_index]
        .set(jnp.arange(route_count, dtype=jnp.int32) // top_count)
    )
    slot_table = slot_token.reshape(expert_count, capacity)
    slice_width = model_width // tp_count
    own_columns = lax.dynamic_slice_in_dim(
        block_normed, lax.axis_index("tp") * slice_width, slice_width, 1
    )
    outgoing = jnp.take(own_columns, slot_table, axis=0, mode="fill", fill_value=0)
    landed = lax.all_to_all(outgoing, "sp", split_axis=0, concat_axis=0, tiled=True)
    arrived = collect(landed, "tp", 2)
    expert_rows = arrived.reshape(-1, model_width)
    gate_part = jnp.dot(expert_rows, expert_gate[0], preferred_element_type=jnp.float32)
    up_part = jnp.dot(expert_rows, expert_up[0], preferred_element_type=jnp.float32)
    inner_act = (jax.nn.silu(gate_part) * up_part).astype(jnp.bfloat16)
    down_width = expert_down.shape[2]
    weight_rows = expert_down[0]
    expert_sum = jnp.dot(
        lax.all_gather(inner_act, "tp", axis=1, tiled=True),
        weight_rows,
        preferred_element_type=jnp.float32,
    )
    expert_out = expert_sum.astype(jnp.bfloat16).reshape(expert_count, capacity, down_width)
    returned = lax.all_to_all(expert_out, "sp", split_axis=0, concat_axis=0, tiled=True)
    per_route = returned.reshape(expert_count * capacity, down_width)[slot_index]
    weighted = per_route.astype(jnp.float32) * route_weight.reshape(-1)[:, None]
    token_sum = jnp.sum(weighted.reshape(tok_count, top_count, down_width), axis=1)
    moe_rows = collect(token_sum.astype(jnp.bfloat16), "tp", 1).astype(token_sum.dtype)
    return (stream + moe_rows).astype(jnp.bfloat16)


def solution(mesh):
    in_specs = (
        P("sp", None),
        P("sp", "tp", None),
        P("sp", "tp", None),
        P("sp", "tp", None),
        P("tp"),
        P(),
        P("tp", None),
        P(),
        P("sp", None, "tp"),
        P("sp", None, "tp"),
        P("sp", None, "tp"),
        P("sp", None),
        P("sp", None),
    )
    out_specs = P("sp", None)
    return jax.shard_map(shards, mesh=mesh, in_specs=in_specs, out_specs=out_specs, check_vma=False)
```

profile of v0, /device:TPU:1, one launch (start us, length us, event | category | flops | bytes accessed | tf_op | source)
XLA Modules:
  0.0 460.8 jit_solution(17257785034887943455)
XLA Ops:
  6.5 1.6 pad_maximum_fusion
  8.2 0.6 slice.25
  8.9 1.0 fusion.59
  10.7 78.0 %all-gather.3.cloned.1.call-done = bf16[8192,2,128]{2,0,1:T(8,128)(2,1)} async-done(((bf16[256,2,128]{2,0,1:T(8,128)(2,1)}), bf16[8192,2,128]{2,0,1:T(8,128)(2,1)}) %all-gather.3.cloned.1.call-update) | async-done | bytes 4194320 | tf_op jit(solution)/shard_map/all_gather | solution.py:17
  88.7 3.8 fusion.58
  92.6 33.3 %while.21 = (s32[]{:T(128)}, f32[1,256]{1,0:T(1,128)S(1)}, f32[1,256]{1,0:T(1,128)S(1)}, f32[256,1,128]{0,2,1:T(8,128)S(1)}, f32[1,256]{1,0:T(1,128)S(1)}, /*ind...) while((s32[]{:T(128)}, f32[1,256]{1,0:T(1,128)S(1)}, ...), condition=%wide.region_7.8_spmd.clone, body=%wide.region_0.7_spmd.clone.sunk | while | flops 102893312 | bytes 4570543 | solution.py:143
  92.6 0.6 dynamic_slice.42
  94.5 2.4 conditional.3
  94.5 0.9 dynamic-slice_bitcast_fusion
  97.0 0.6 dynamic_slice.42
  98.9 0.6 dynamic_slice.42
  100.8 0.6 dynamic_slice.42
  102.8 0.6 dynamic_slice.42
  104.7 0.6 dynamic_slice.42
  106.6 0.6 dynamic_slice.42
  108.6 0.6 dynamic_slice.42
  110.5 0.6 dynamic_slice.42
  112.4 0.6 dynamic_slice.42
  114.4 0.6 dynamic_slice.42
  116.3 0.6 dynamic_slice.42
  118.2 0.6 dynamic_slice.42
  120.2 0.6 dynamic_slice.42
  122.1 0.6 dynamic_slice.42
  126.0 2.5 convolution_convert_fusion
  128.6 6.5 %all-to-all-start = ((bf16[16,16,2048]{2,1,0:T(8,128)(2,1)}), bf16[16,16,2048]{2,1,0:T(8,128)(2,1)S(1)}, u32[]{:S(2)}, u32[]{:S(2)}) async-start(bf16[16,16,2048]{2,1,0:T(8,128)(2,1)} %bitcast.29), calls=%async_computation | async-start | bytes 2097152 | tf_op jit(solution)/shard_map/all_to_all | solution.py:27
  135.6 1.2 reduce-window.6
  137.4 14.1 %all-to-all-done = bf16[16,16,2048]{2,1,0:T(8,128)(2,1)S(1)} async-done(((bf16[16,16,2048]{2,1,0:T(8,128)(2,1)}), bf16[16,16,2048]{2,1,0:T(8,128)(2,1)S(1)}, u32[]{:S(2)}, u32[]{:S(2)}) %all-to-all-start) | async-done | bytes 1048608 | tf_op jit(solution)/shard_map/all_to_all | solution.py:27
  151.7 1.1 broadcast_in_dim.38
  152.8 4.5 all-to-all-start.1
  157.4 2.4 scatter_custom_fusion
  160.0 0.8 dynamic-slice
  160.8 12.4 %all-to-all-done.1 = bf16[16,16,2048]{2,1,0:T(8,128)(2,1)S(1)} async-done(((bf16[16,16,2048]{2,1,0:T(8,128)(2,1)}), bf16[16,16,2048]{2,1,0:T(8,128)(2,1)S(1)}, u32[]{:S(2)}, u32[]{:S(2)}) %all-to-all-start.1) | async-done | bytes 1048608 | tf_op jit(solution)/shard_map/all_to_all | solution.py:38
  173.7 3.2 gather_fusion
  177.2 65.0 %all_to_all.30 = bf16[32,32,128]{2,1,0:T(8,128)(2,1)S(1)} all-to-all(bf16[32,32,128]{2,1,0:T(8,128)(2,1)S(1)} %broadcast_select_fusion), channel_id=1, replica_groups=mesh['sp'=32,'tp'=16] {'sp'}, dimensions={0} | all-to-all | bytes 524288 | tf_op jit(solution)/shard_map/all_to_all | solution.py:187
  242.1 0.8 broadcast_in_dim.42
  242.9 52.7 %all_to_all.31 = bf16[16,32,32,128]{3,2,1,0:T(8,128)(2,1)S(1)} all-to-all(bf16[16,32,32,128]{3,2,1,0:T(8,128)(2,1)S(1)} %broadcast_in_dim.42), channel_id=1, replica_groups=mesh['sp'=32,'tp'=16] {'tp'}, dimensions={0} | all-to-all | bytes 8388608 | tf_op jit(solution)/shard_map/all_to_all | solution.py:38
  295.6 4.9 %copy.34 = bf16[32,32,16,128]{3,2,1,0:T(8,128)(2,1)S(1)} copy(bf16[32,32,16,128]{3,1,0,2:T(8,128)(2,1)S(1)} %bitcast.139) | data formatting | bytes 8388608 | tf_op jit(solution)/shard_map/transpose | solution.py:44
  300.5 1.3 fusion.26
  301.8 2.1 fusion.34
  303.9 81.9 %all-gather.5.cloned.1.call-done = bf16[1024,4096]{1,0:T(8,128)(2,1)} async-done(((bf16[1024,256]{1,0:T(8,128)(2,1)}), bf16[1024,4096]{1,0:T(8,128)(2,1)}) %all-gather.5.cloned.1.call-update) | async-done | bytes 8388624 | tf_op jit(solution)/shard_map/all_gather | solution.py:196
  385.8 6.6 %convolution_convert_fusion.1 = bf16[1024,128]{1,0:T(8,128)(2,1)} fusion(bf16[1024,4096]{1,0:T(8,128)(2,1)} %all-gather.5.cloned.1.call-done, bf16[1,4096,128]{2,1,0:T(8,128)(2,1)} %param.27), kind=kOutput, calls=%fused_computation.53 | convolution fusion | flops 1073872896 | bytes 9699328 | tf_op jit(solution)/shard_map/dot_general | solution.py:195
  392.4 14.4 %all-to-all-start.4 = ((bf16[32,32,128]{2,1,0:T(8,128)(2,1)}), bf16[32,32,128]{2,1,0:T(8,128)(2,1)S(1)}, u32[]{:S(2)}, u32[]{:S(2)}) async-start(bf16[32,32,128]{2,1,0:T(8,128)(2,1)} %bitcast.151), calls=%async_computation.4 | async-start | bytes 524288 | tf_op jit(solution)/shard_map/all_to_all | solution.py:201
  406.8 0.8 copy.35
  407.6 21.5 %all-to-all-done.4 = bf16[32,32,128]{2,1,0:T(8,128)(2,1)S(1)} async-done(((bf16[32,32,128]{2,1,0:T(8,128)(2,1)}), bf16[32,32,128]{2,1,0:T(8,128)(2,1)S(1)}, u32[]{:S(2)}, u32[]{:S(2)}) %all-to-all-start.4) | async-done | bytes 262176 | tf_op jit(solution)/shard_map/all_to_all | solution.py:201
  429.1 1.3 gather_fusion.1
  430.4 1.3 fusion.40
  432.0 20.5 %all_to_all.32 = bf16[16,256,128]{2,1,0:T(8,128)(2,1)S(1)} all-to-all(bf16[16,256,128]{2,1,0:T(8,128)(2,1)S(1)} %broadcast_in_dim.43), channel_id=1, replica_groups=mesh['sp'=32,'tp'=16] {'tp'}, dimensions={0} | all-to-all | bytes 2097152 | tf_op jit(solution)/shard_map/all_to_all | solution.py:38
  452.5 1.5 fusion.30
  (115 shorter events, 5.1 us)
Async XLA Ops:
  6.5 294.0 %copy-start = (bf16[1,2048,256]{2,1,0:T(8,128)(2,1)S(1)}, bf16[1,2048,256]{2,1,0:T(8,128)(2,1)}, u32[]{:S(2)}) copy-start(bf16[1,2048,256]{2,1,0:T(8,128)(2,1)} %param.25) | copy-start | bytes 3145732
  6.5 82.2 %all-gather.3.cloned.1.call-start = ((), (), s32[]{:S(2)}) async-start(), calls=%async_computation.6 | async-start | bytes 4325376 | tf_op jit(solution)/shard_map/all_gather | solution.py:17
  92.6 33.4 %copy-start.4 = (f32[128]{0:T(128)S(1)}, f32[128]{0:T(128)}, u32[]{:S(2)}) copy-start(f32[128]{0:T(128)} %param.22) | copy-start | bytes 1540
  126.0 9.2 %copy-start.2 = (s32[256,2]{0,1:T(2,128)S(1)}, s32[256,2]{0,1:T(2,128)}, u32[]{:S(2)}) copy-start(s32[256,2]{0,1:T(2,128)} %param.28) | copy-start | bytes 6148
  128.6 23.0 %all-to-all-start = ((bf16[16,16,2048]{2,1,0:T(8,128)(2,1)}), bf16[16,16,2048]{2,1,0:T(8,128)(2,1)S(1)}, u32[]{:S(2)}, u32[]{:S(2)}) async-start(bf16[16,16,2048]{2,1,0:T(8,128)(2,1)} %bitcast.29), calls=%async_computation | async-start | bytes 2097152 | tf_op jit(solution)/shard_map/all_to_all | solution.py:27
  137.4 35.8 %copy-start.1 = (bf16[256,2048]{1,0:T(8,128)(2,1)S(1)}, bf16[256,2048]{1,0:T(8,128)(2,1)}, u32[]{:S(2)}) copy-start(bf16[256,2048]{1,0:T(8,128)(2,1)} %param.17) | copy-start | bytes 3145732
  152.8 20.4 %all-to-all-start.1 = ((bf16[16,16,2048]{2,1,0:T(8,128)(2,1)}), bf16[16,16,2048]{2,1,0:T(8,128)(2,1)S(1)}, u32[]{:S(2)}, u32[]{:S(2)}) async-start(bf16[16,16,2048]{2,1,0:T(8,128)(2,1)} %broadcast_in_dim.38), calls=%async_computation.1 | async-start | bytes 2097152 | tf_op jit(solution)/shard_map/all_to_all | solution.py:38
  157.3 228.5 %all-gather.5.cloned.1.call-start = ((), (), s32[]{:S(2)}) async-start(), calls=%async_computation.7 | async-start | bytes 8912896 | tf_op jit(solution)/shard_map/all_gather | solution.py:196
  300.5 1.3 copy-start.5
  303.9 102.9 %copy-start.3 = (f32[256,2]{0,1:T(2,128)S(1)}, f32[256,2]{0,1:T(2,128)}, u32[]{:S(2)}) copy-start(f32[256,2]{0,1:T(2,128)} %param.29) | copy-start | bytes 6148
  392.4 36.6 %all-to-all-start.4 = ((bf16[32,32,128]{2,1,0:T(8,128)(2,1)}), bf16[32,32,128]{2,1,0:T(8,128)(2,1)S(1)}, u32[]{:S(2)}, u32[]{:S(2)}) async-start(bf16[32,32,128]{2,1,0:T(8,128)(2,1)} %bitcast.151), calls=%async_computation.4 | async-start | bytes 524288 | tf_op jit(solution)/shard_map/all_to_all | solution.py:201
Sparse Core Ops, SparseCore 0:
  9.5 79.1 all-gather.2
  304.0 81.7 all-gather.4
where the time goes:
time: 462 us; the launch traced here: 461 us
  waiting for transfers between devices  208 us (45%)
  blocking collectives  138 us (30%)
  local copies, waits for them, and re-layouts  32.7 us (7%)
  starting transfers between devices  25.4 us (5%)
  loops' own time  21.5 us (5%)
  between operations  14.4 us (3%)
  matrix products  13.6 us (3%)
  other arithmetic  7.04 us (2%)
    all_gather x1, waiting for transfers between devices, shards(): lax.all_gather(inner_act, 'tp', axis=1, tiled=True)  81.9 us
    all_gather x1, waiting for transfers between devices, sent_together(): lax.all_gather(both, axis, axis=dim, tiled=True)  78 us
    all_to_all x2, blocking collectives, from_everyone(): lax.all_to_all(jnp.broadcast_to(array[None], (peers, *array.shape)), axis...  73.2 us
    all_to_all x1, blocking collectives, shards(): lax.all_to_all(outgoing, 'sp', split_axis=0, concat_axis=0, tiled=True)  65 us
    all_to_all x1, waiting for transfers between devices, shards(): lax.all_to_all(expert_out, 'sp', split_axis=0, concat_axis=0, tiled=True)  21.5 us
    another operation x1, loops' own time, shards(): lax.scan(visit, running, (jnp.arange(block_count, dtype=jnp.int32), key_b...  21.2 us
    all_to_all x1, starting transfers between devices, shards(): lax.all_to_all(expert_out, 'sp', split_axis=0, concat_axis=0, tiled=True)  14.4 us
    all_to_all x1, waiting for transfers between devices, sum_at_owner(): lax.all_to_all(parts, axis, split_axis=0, concat_axis=0, tiled=True)  14.1 us
  transfers between devices with their start and end apart: 5, of which 5 were waited for; matrix products, arithmetic and copies ran while one was open for 2% of the time, Pallas kernels for 0%

commit v1 on v0

--- a/solution.py
+++ b/solution.py
@@ -6,6 +6,12 @@
 
 GROUPS = 4
 norm_eps = 1e-06
+
+
+def gather_by_exchange(x, axis, dim):
+    size = lax.axis_size(axis)
+    repeats = [size if d == dim else 1 for d in range(x.ndim)]
+    return lax.all_to_all(jnp.tile(x, repeats), axis, split_axis=dim, concat_axis=dim, tiled=True)
 
 
 def sent_together(arrays, axis, dim, along):
@@ -193,9 +199,7 @@
     down_width = expert_down.shape[2]
     weight_rows = expert_down[0]
     expert_sum = jnp.dot(
-        lax.all_gather(inner_act, "tp", axis=1, tiled=True),
-        weight_rows,
-        preferred_element_type=jnp.float32,
+        gather_by_exchange(inner_act, "tp", 1), weight_rows, preferred_element_type=jnp.float32
     )
     expert_out = expert_sum.astype(jnp.bfloat16).reshape(expert_count, capacity, down_width)
     returned = lax.all_to_all(expert_out, "sp", split_axis=0, concat_axis=0, tiled=True)

time: 462 us -> 482 us (1.043)
  blocking collectives: 138 us -> 235 us
  waiting for transfers between devices: 208 us -> 126 us
  local copies, waits for them, and re-layouts: 32.7 us -> 45.8 us
  starting transfers between devices: 25.4 us -> 17.7 us
    all_to_all x0 -> x1, blocking collectives: none -> 98.3 us  [gather_by_exchange(): lax.all_to_all(jnp.tile(x, repeats), axis, split_axis=dim, concat_axis=di...]
    all_gather x1 -> x0, waiting for transfers between devices: 81.9 us -> none  [shards(): lax.all_gather(inner_act, 'tp', axis=1, tiled=True)]
    all_to_all x0 -> x1, local copies, waits for them, and re-layouts: none -> 12.3 us  [gather_by_exchange(): lax.all_to_all(jnp.tile(x, repeats), axis, split_axis=dim, concat_axis=di...]
    all_to_all x1, starting transfers between devices: 14.4 us -> 6.73 us  [shards(): lax.all_to_all(expert_out, 'sp', split_axis=0, concat_axis=0, tiled=True)]
  transfers between devices with their start and end apart: 5 -> 4, of which waited for: 5 -> 4; matrix products, arithmetic and copies ran while one was open for 2% -> 2% of each run, Pallas kernels for 0% -> 0%
where the time goes in v1:
time: 482 us; the launch traced here: 480 us
  blocking collectives  235 us (49%)
  waiting for transfers between devices  126 us (26%)
  local copies, waits for them, and re-layouts  45.8 us (10%)
  loops' own time  21.5 us (4%)
  starting transfers between devices  17.7 us (4%)
  between operations  14.4 us (3%)
  matrix products  12.9 us (3%)
  other arithmetic  7.04 us (1%)
    all_to_all x1, blocking collectives, gather_by_exchange(): lax.all_to_all(jnp.tile(x, repeats), axis, split_axis=dim, concat_axis=di...  98.3 us
    all_gather x1, waiting for transfers between devices, sent_together(): lax.all_gather(both, axis, axis=dim, tiled=True)  78 us
    all_to_all x2, blocking collectives, from_everyone(): lax.all_to_all(jnp.broadcast_to(array[None], (peers, *array.shape)), axis...  71.4 us
    all_to_all x1, blocking collectives, shards(): lax.all_to_all(outgoing, 'sp', split_axis=0, concat_axis=0, tiled=True)  64.9 us
    all_to_all x1, waiting for transfers between devices, shards(): lax.all_to_all(expert_out, 'sp', split_axis=0, concat_axis=0, tiled=True)  21.5 us
    another operation x1, loops' own time, shards(): lax.scan(visit, running, (jnp.arange(block_count, dtype=jnp.int32), key_b...  21.2 us
    all_to_all x1, waiting for transfers between devices, sum_at_owner(): lax.all_to_all(parts, axis, split_axis=0, concat_axis=0, tiled=True)  14.1 us
    all_to_all x1, waiting for transfers between devices, from_everyone(): lax.all_to_all(jnp.broadcast_to(array[None], (peers, *array.shape)), axis...  12.4 us
  transfers between devices with their start and end apart: 4, of which 4 were waited for; matrix products, arithmetic and copies ran while one was open for 2% of the time, Pallas kernels for 0%

profile of v1, /device:TPU:1, one launch (start us, length us, event | category | flops | bytes accessed | tf_op | source)
XLA Modules:
  0.0 480.1 jit_solution(16894597995826434151)
XLA Ops:
  6.5 1.6 pad_maximum_fusion
  8.2 0.6 slice.25
  8.9 1.0 fusion.59
  10.7 78.0 %all-gather.2.cloned.1.call-done = bf16[8192,2,128]{2,0,1:T(8,128)(2,1)} async-done(((bf16[256,2,128]{2,0,1:T(8,128)(2,1)}), bf16[8192,2,128]{2,0,1:T(8,128)(2,1)}) %all-gather.2.cloned.1.call-update) | async-done | bytes 4194320 | tf_op jit(solution)/shard_map/all_gather | solution.py:23
  88.7 3.8 fusion.58
  92.6 33.3 %while.21 = (s32[]{:T(128)}, f32[1,256]{1,0:T(1,128)S(1)}, f32[1,256]{1,0:T(1,128)S(1)}, f32[256,1,128]{0,2,1:T(8,128)S(1)}, f32[1,256]{1,0:T(1,128)S(1)}, /*ind...) while((s32[]{:T(128)}, f32[1,256]{1,0:T(1,128)S(1)}, ...), condition=%wide.region_7.8_spmd.clone, body=%wide.region_0.7_spmd.clone.sunk | while | flops 102893312 | bytes 4570543 | solution.py:149
  92.6 0.6 dynamic_slice.42
  94.5 2.4 conditional.3
  94.5 0.9 dynamic-slice_bitcast_fusion
  97.0 0.6 dynamic_slice.42
  98.9 0.6 dynamic_slice.42
  100.8 0.6 dynamic_slice.42
  102.8 0.6 dynamic_slice.42
  104.7 0.6 dynamic_slice.42
  106.6 0.6 dynamic_slice.42
  108.6 0.6 dynamic_slice.42
  110.5 0.6 dynamic_slice.42
  112.4 0.6 dynamic_slice.42
  114.4 0.6 dynamic_slice.42
  116.3 0.6 dynamic_slice.42
  118.2 0.6 dynamic_slice.42
  126.1 2.5 convolution_convert_fusion
  128.6 6.5 %all-to-all-start = ((bf16[16,16,2048]{2,1,0:T(8,128)(2,1)}), bf16[16,16,2048]{2,1,0:T(8,128)(2,1)S(1)}, u32[]{:S(2)}, u32[]{:S(2)}) async-start(bf16[16,16,2048]{2,1,0:T(8,128)(2,1)} %bitcast.29), calls=%async_computation | async-start | bytes 2097152 | tf_op jit(solution)/shard_map/all_to_all | solution.py:33
  135.6 1.2 reduce-window.6
  137.4 14.1 %all-to-all-done = bf16[16,16,2048]{2,1,0:T(8,128)(2,1)S(1)} async-done(((bf16[16,16,2048]{2,1,0:T(8,128)(2,1)}), bf16[16,16,2048]{2,1,0:T(8,128)(2,1)S(1)}, u32[]{:S(2)}, u32[]{:S(2)}) %all-to-all-start) | async-done | bytes 1048608 | tf_op jit(solution)/shard_map/all_to_all | solution.py:33
  151.7 1.1 broadcast_in_dim.38
  152.8 4.5 all-to-all-start.1
  157.3 2.4 scatter_custom_fusion
  160.0 0.8 dynamic-slice
  160.8 12.4 %all-to-all-done.1 = bf16[16,16,2048]{2,1,0:T(8,128)(2,1)S(1)} async-done(((bf16[16,16,2048]{2,1,0:T(8,128)(2,1)}), bf16[16,16,2048]{2,1,0:T(8,128)(2,1)S(1)}, u32[]{:S(2)}, u32[]{:S(2)}) %all-to-all-start.1) | async-done | bytes 1048608 | tf_op jit(solution)/shard_map/all_to_all | solution.py:44
  173.7 3.2 gather_fusion
  177.2 64.9 %all_to_all.39 = bf16[32,32,128]{2,1,0:T(8,128)(2,1)S(1)} all-to-all(bf16[32,32,128]{2,1,0:T(8,128)(2,1)S(1)} %broadcast_select_fusion), channel_id=1, replica_groups=mesh['sp'=32,'tp'=16] {'sp'}, dimensions={0} | all-to-all | bytes 524288 | tf_op jit(solution)/shard_map/all_to_all | solution.py:193
  242.1 0.8 broadcast_in_dim.42
  242.9 52.7 %all_to_all.40 = bf16[16,32,32,128]{3,2,1,0:T(8,128)(2,1)S(1)} all-to-all(bf16[16,32,32,128]{3,2,1,0:T(8,128)(2,1)S(1)} %broadcast_in_dim.42), channel_id=1, replica_groups=mesh['sp'=32,'tp'=16] {'tp'}, dimensions={0} | all-to-all | bytes 8388608 | tf_op jit(solution)/shard_map/all_to_all | solution.py:44
  295.6 4.9 %copy.45 = bf16[32,32,16,128]{3,2,1,0:T(8,128)(2,1)S(1)} copy(bf16[32,32,16,128]{3,1,0,2:T(8,128)(2,1)S(1)} %bitcast.140) | data formatting | bytes 8388608 | tf_op jit(solution)/shard_map/transpose | solution.py:50
  300.5 1.3 fusion.26
  301.8 1.3 fusion.34
  303.1 0.8 tile.2
  303.9 98.3 %all_to_all.41 = bf16[1024,16,256]{2,0,1:T(8,128)(2,1)} all-to-all(bf16[1024,16,256]{2,0,1:T(8,128)(2,1)S(1)} %tile.2), channel_id=1, replica_groups=mesh['sp'=32,'tp'=16] {'tp'}, dimensions={1} | all-to-all | bytes 16777216 | tf_op jit(solution)/shard_map/all_to_all | solution.py:14
  402.2 12.3 %copy.46 = bf16[1024,16,256]{0,2,1:T(8,128)(2,1)} copy(bf16[1024,16,256]{2,0,1:T(8,128)(2,1)} %all_to_all.41) | data formatting | bytes 16777216 | tf_op jit(solution)/shard_map/all_to_all | solution.py:14
  414.5 6.7 %convolution_convert_fusion.1 = bf16[1024,128]{1,0:T(8,128)(2,1)} fusion(bf16[1024,4096]{0,1:T(8,128)(2,1)} %bitcast.141, bf16[1,4096,128]{2,1,0:T(8,128)(2,1)} %param.27), kind=kOutput, calls=%fused_computation.53 | convolution fusion | flops 1073872896 | bytes 9699328 | tf_op jit(solution)/shard_map/dot_general | solution.py:201
  421.2 6.7 %all-to-all-start.5 = ((bf16[32,32,128]{2,1,0:T(8,128)(2,1)}), bf16[32,32,128]{2,1,0:T(8,128)(2,1)S(1)}, u32[]{:S(2)}, u32[]{:S(2)}) async-start(bf16[32,32,128]{2,1,0:T(8,128)(2,1)} %bitcast.153), calls=%async_computation.5 | async-start | bytes 524288 | tf_op jit(solution)/shard_map/all_to_all | solution.py:205
  428.0 0.8 copy.47
  428.7 21.5 %all-to-all-done.5 = bf16[32,32,128]{2,1,0:T(8,128)(2,1)S(1)} async-done(((bf16[32,32,128]{2,1,0:T(8,128)(2,1)}), bf16[32,32,128]{2,1,0:T(8,128)(2,1)S(1)}, u32[]{:S(2)}, u32[]{:S(2)}) %all-to-all-start.5) | async-done | bytes 262176 | tf_op jit(solution)/shard_map/all_to_all | solution.py:205
  450.2 1.3 gather_fusion.1
  451.5 1.3 fusion.40
  453.1 18.7 %all_to_all.42 = bf16[16,256,128]{2,1,0:T(8,128)(2,1)S(1)} all-to-all(bf16[16,256,128]{2,1,0:T(8,128)(2,1)S(1)} %broadcast_in_dim.43), channel_id=1, replica_groups=mesh['sp'=32,'tp'=16] {'tp'}, dimensions={0} | all-to-all | bytes 2097152 | tf_op jit(solution)/shard_map/all_to_all | solution.py:44
  471.8 1.5 fusion.30
  (115 shorter events, 6.2 us)
Async XLA Ops:
  6.5 293.9 %copy-start = (bf16[1,2048,256]{2,1,0:T(8,128)(2,1)S(1)}, bf16[1,2048,256]{2,1,0:T(8,128)(2,1)}, u32[]{:S(2)}) copy-start(bf16[1,2048,256]{2,1,0:T(8,128)(2,1)} %param.25) | copy-start | bytes 3145732
  6.5 82.2 %all-gather.2.cloned.1.call-start = ((), (), s32[]{:S(2)}) async-start(), calls=%async_computation.7 | async-start | bytes 4325376 | tf_op jit(solution)/shard_map/all_gather | solution.py:23
  92.6 33.4 %copy-start.4 = (f32[128]{0:T(128)S(1)}, f32[128]{0:T(128)}, u32[]{:S(2)}) copy-start(f32[128]{0:T(128)} %param.22) | copy-start | bytes 1540
  126.0 9.2 %copy-start.2 = (s32[256,2]{0,1:T(2,128)S(1)}, s32[256,2]{0,1:T(2,128)}, u32[]{:S(2)}) copy-start(s32[256,2]{0,1:T(2,128)} %param.28) | copy-start | bytes 6148
  128.6 23.0 %all-to-all-start = ((bf16[16,16,2048]{2,1,0:T(8,128)(2,1)}), bf16[16,16,2048]{2,1,0:T(8,128)(2,1)S(1)}, u32[]{:S(2)}, u32[]{:S(2)}) async-start(bf16[16,16,2048]{2,1,0:T(8,128)(2,1)} %bitcast.29), calls=%async_computation | async-start | bytes 2097152 | tf_op jit(solution)/shard_map/all_to_all | solution.py:33
  137.4 35.8 %copy-start.1 = (bf16[256,2048]{1,0:T(8,128)(2,1)S(1)}, bf16[256,2048]{1,0:T(8,128)(2,1)}, u32[]{:S(2)}) copy-start(bf16[256,2048]{1,0:T(8,128)(2,1)} %param.17) | copy-start | bytes 3145732
  152.8 20.4 %all-to-all-start.1 = ((bf16[16,16,2048]{2,1,0:T(8,128)(2,1)}), bf16[16,16,2048]{2,1,0:T(8,128)(2,1)S(1)}, u32[]{:S(2)}, u32[]{:S(2)}) async-start(bf16[16,16,2048]{2,1,0:T(8,128)(2,1)} %broadcast_in_dim.38), calls=%async_computation.1 | async-start | bytes 2097152 | tf_op jit(solution)/shard_map/all_to_all | solution.py:44
  300.5 1.3 copy-start.5
  414.5 13.5 %copy-start.3 = (f32[256,2]{0,1:T(2,128)S(1)}, f32[256,2]{0,1:T(2,128)}, u32[]{:S(2)}) copy-start(f32[256,2]{0,1:T(2,128)} %param.29) | copy-start | bytes 6148
  421.2 29.0 %all-to-all-start.5 = ((bf16[32,32,128]{2,1,0:T(8,128)(2,1)}), bf16[32,32,128]{2,1,0:T(8,128)(2,1)S(1)}, u32[]{:S(2)}, u32[]{:S(2)}) async-start(bf16[32,32,128]{2,1,0:T(8,128)(2,1)} %bitcast.153), calls=%async_computation.5 | async-start | bytes 524288 | tf_op jit(solution)/shard_map/all_to_all | solution.py:205
Sparse Core Ops, SparseCore 0:
  9.5 79.1 all-gather.1
